TPU v7x, 32 devices: a whole 2x2x4 slice. The times are simulated.
32 devices in a mesh: tp: 8 (over z, x), dp: 4 (over y, core).
Axes of the slice: x: 2, y: 2, z: 4, core: 2. Of those that a mesh axis runs over, the one named last changes fastest.
Arguments:
- tokens: bfloat16 [128, 4096], P('tp', 'dp'), may hold values from -6 to 6
- query_weight: bfloat16 [2, 4096, 2048], P(None, 'dp', 'tp'), may hold values from -0.09375 to 0.09375
- key_weight: bfloat16 [2, 4096, 2048], P(None, 'dp', 'tp'), may hold values from -0.09375 to 0.09375
- value_weight: bfloat16 [2, 4096, 2048], P(None, 'dp', 'tp'), may hold values from -0.09375 to 0.09375
- outgate_weight: bfloat16 [2, 4096, 2048], P(None, 'dp', 'tp'), may hold values from -0.09375 to 0.09375
- igate_weight: bfloat16 [2, 4096, 16], replicated, may hold values from -0.09375 to 0.09375
- fgate_weight: bfloat16 [2, 4096, 16], replicated, may hold values from -0.09375 to 0.09375
- norm_gain: float32 [2, 4096], P(None, 'dp'), may hold values from 0.1 to 1.9
- head_gain: float32 [2, 2048], P(None, 'tp'), may hold values from 0.1 to 1.9
- proj_weight: bfloat16 [2, 2048, 4096], P(None, 'tp', 'dp'), may hold values from -0.125 to 0.125
- cell_state: float32 [2, 128, 16, 128, 128], P(None, 'dp', 'tp'), may hold values from -1.8 to 1.8
- normer_state: float32 [2, 128, 16, 128], P(None, 'dp', 'tp'), may hold values from -1.8 to 1.8
- stab_state: float32 [2, 128, 16], P(None, 'dp', 'tp'), may hold values from -4 to 4
Outputs:
- final_rows: bfloat16 [128, 4096], P('tp', 'dp')
- cell_out: float32 [2, 128, 16, 128, 128], P(None, 'dp', 'tp')
- normer_out: float32 [2, 128, 16, 128], P(None, 'dp', 'tp')
- stab_out: float32 [2, 128, 16], P(None, 'dp', 'tp')
All inputs are finite; a program needn't handle non-finite values.
Results may differ from a plain program's by a relative error of at most 0.012.
The roundings to bfloat16 on the way count: a program that leaves them out, or rounds other values in their place, can miss the bound.
Values may be sent and summed in bfloat16 or wider, within the bound.
No kernel may reach another device: no remote copies, remote signals or barrier semaphores. Data moves between devices by JAX's collectives and lax.ppermute only.
A program may use at most 64 MiB of HBM per device.

v0:
```python
import jax
import jax.numpy as jnp
from jax import lax
from jax.sharding import PartitionSpec as P

D = 4096
EPSILON = 1e-06


def gather_rows(block_input):
    return lax.all_gather(block_input, "tp", axis=0, tiled=True)


def spread_heads(out_part):
    return lax.psum_scatter(out_part, "tp", scatter_dimension=0, tiled=True)


def per_device(
    tokens,
    query_weight,
    key_weight,
    value_weight,
    outgate_weight,
    igate_weight,
    fgate_weight,
    norm_gain,
    head_gain,
    proj_weight,
    cell_state,
    normer_state,
    stab_state,
):
    dp_rank = lax.axis_index("dp")
    tp_rank = lax.axis_index("tp")
    local_seqs = cell_state.shape[1]
    local_heads = cell_state.shape[2]
    head_dim = cell_state.shape[3]
    row_width = query_weight.shape[1]
    num_blocks = query_weight.shape[0]
    gathered = gather_rows(tokens)
    final_rows = tokens
    cell_list = []
    normer_list = []
    stab_list = []
    for layer_num in range(num_blocks):
        as_float = gathered.astype(jnp.float32)
        part_squares = jnp.sum(as_float * as_float, axis=1)
        scaled = (as_float * norm_gain[layer_num]).astype(jnp.bfloat16)

        def product(weight):
            return jnp.dot(scaled, weight, preferred_element_type=jnp.float32)

        gate_start = (dp_rank * row_width, tp_rank * local_heads)
        igate_rows = lax.dynamic_slice(
            igate_weight[layer_num], gate_start, (row_width, local_heads)
        )
        fgate_rows = lax.dynamic_slice(
            fgate_weight[layer_num], gate_start, (row_width, local_heads)
        )
        query_part = product(query_weight[layer_num])
        key_part = product(key_weight[layer_num])
        value_part = product(value_weight[layer_num])
        outgate_part = product(outgate_weight[layer_num])
        igate_part = product(igate_rows)
        forget_part = product(fgate_rows)
        query_sum, key_sum, value_sum, outgate_sum, igate_sum, forget_sum = (
            lax.psum_scatter(query_part, "dp", scatter_dimension=0, tiled=True),
            lax.psum_scatter(key_part, "dp", scatter_dimension=0, tiled=True),
            lax.psum_scatter(value_part, "dp", scatter_dimension=0, tiled=True),
            lax.psum_scatter(outgate_part, "dp", scatter_dimension=0, tiled=True),
            lax.psum_scatter(igate_part, "dp", scatter_dimension=0, tiled=True),
            lax.psum_scatter(forget_part, "dp", scatter_dimension=0, tiled=True),
        )
        total_sq = lax.psum(part_squares, "dp")
        own_sq = lax.dynamic_slice_in_dim(total_sq, dp_rank * local_seqs, local_seqs)
        inv_rms = lax.rsqrt(own_sq / D + EPSILON)[:, None]
        query_rows = (query_sum * inv_rms).reshape(local_seqs, local_heads, head_dim)
        key_rows = (key_sum * inv_rms * head_dim ** (-0.5)).reshape(
            local_seqs, local_heads, head_dim
        )
        value_rows = (value_sum * inv_rms).reshape(local_seqs, local_heads, head_dim)
        outgate = outgate_sum * inv_rms
        igate = igate_sum * inv_rms
        forget = jax.nn.log_sigmoid(forget_sum * inv_rms)
        prev_stab = stab_state[layer_num]
        new_stab = jnp.maximum(forget + prev_stab, igate)
        keep_rate = jnp.exp(forget + prev_stab - new_stab)
        write_rate = jnp.exp(igate - new_stab)
        new_cell = (
            keep_rate[..., None, None] * cell_state[layer_num]
            + write_rate[..., None, None] * value_rows[..., :, None] * key_rows[..., None, :]
        )
        new_normer = (
            keep_rate[..., None] * normer_state[layer_num] + write_rate[..., None] * key_rows
        )
        numerator = jnp.einsum(
            "bhvd,bhd->bhv", new_cell, query_rows, precision=lax.Precision.HIGHEST
        )
        denominator = jnp.maximum(jnp.abs(jnp.sum(new_normer * query_rows, axis=-1)), 1.0)
        readout = numerator / denominator[..., None]
        normed = readout * lax.rsqrt(jnp.mean(readout * readout, axis=-1, keepdims=True) + EPSILON)
        normed = normed * head_gain[layer_num].reshape(local_heads, head_dim)
        gated_out = (
            jax.nn.sigmoid(outgate) * normed.reshape(local_seqs, local_heads * head_dim)
        ).astype(jnp.bfloat16)
        all_gated = lax.all_gather(gated_out, "dp", axis=0, tiled=True)
        out_part = jnp.dot(all_gated, proj_weight[layer_num], preferred_element_type=jnp.float32)
        if layer_num + 1 < num_blocks:
            gathered = lax.psum(out_part, "tp").astype(jnp.bfloat16)
        else:
            final_rows = spread_heads(out_part).astype(jnp.bfloat16)
        cell_list.append(new_cell)
        normer_list.append(new_normer)
        stab_list.append(new_stab)
    return (final_rows, jnp.stack(cell_list), jnp.stack(normer_list), jnp.stack(stab_list))


def solution(mesh):
    return jax.shard_map(
        per_device,
        mesh=mesh,
        in_specs=(
            P("tp", "dp"),
            P(None, "dp", "tp"),
            P(None, "dp", "tp"),
            P(None, "dp", "tp"),
            P(None, "dp", "tp"),
            P(),
            P(),
            P(None, "dp"),
            P(None, "tp"),
            P(None, "tp", "dp"),
            P(None, "dp", "tp", None, None),
            P(None, "dp", "tp", None),
            P(None, "dp", "tp"),
        ),
        out_specs=(
            P("tp", "dp"),
            P(None, "dp", "tp", None, None),
            P(None, "dp", "tp", None),
            P(None, "dp", "tp"),
        ),
        check_vma=False,
    )
```

profile of v0, /device:TPU:0, one launch (start us, length us, event | category | flops | bytes accessed | tf_op | source)
XLA Modules:
  0.0 431.7 jit_solution(14644992044606748619)
XLA Ops:
  7.3 0.9 fusion.90
  8.1 32.8 %all_gather.9 = bf16[128,1024]{1,0:T(8,128)(2,1)S(1)} all-gather(bf16[16,1024]{1,0:T(8,128)(2,1)} %param.13), channel_id=1, replica_groups=mesh['tp'=8,'dp'=4] {'tp'}, dimensions={0}, use_global_device_ids=true | all-gather | bytes 294912 | tf_op jit(solution)/shard_map/all_gather | solution.py:11
  40.9 1.6 fusion.89
  42.5 0.9 fusion.53
  43.5 1.6 fusion.88
  45.2 0.9 fusion.55
  46.1 1.9 fusion.36
  48.1 1.9 fusion.34
  50.2 0.9 fusion.32
  51.1 0.9 fusion.38
  52.3 5.7 %psum.21 = f32[128]{0:T(128)S(1)} all-reduce(f32[128]{0:T(128)S(1)} %fusion.17), channel_id=1, replica_groups=mesh['tp'=8,'dp'=4] {'dp'}, use_global_device_ids=true, to_apply=%region_2.0 | all-reduce | flops 128 | bytes 1024 | tf_op jit(solution)/shard_map/psum | solution.py:74
  58.0 6.2 %reduce-scatter.42.cloned.1.call-done = f32[32,2]{1,0:T(8,128)} async-done(((f32[128,2]{1,0:T(8,128)}), f32[32,2]{1,0:T(8,128)}) %reduce-scatter.42.cloned.1.call-update) | async-done | bytes 272
  64.2 0.8 copy.48
  65.0 21.2 %reduce-scatter.40.cloned.1.call-done = f32[32,2]{1,0:T(8,128)} async-done(((f32[128,2]{1,0:T(8,128)}), f32[32,2]{1,0:T(8,128)}) %reduce-scatter.40.cloned.1.call-update) | async-done | bytes 272
  86.2 0.8 copy.46
  87.2 21.6 %reduce-scatter.24.cloned.1.call-done = f32[32,256]{1,0:T(8,128)} async-done(((f32[128,256]{1,0:T(8,128)}), f32[32,256]{1,0:T(8,128)}) %reduce-scatter.24.cloned.1.call-update) | async-done | bytes 32784 | tf_op jit(solution)/shard_map/reduce_scatter | solution.py:69
  108.9 21.9 %reduce-scatter.26.cloned.1.call-done = f32[32,256]{1,0:T(8,128)} async-done(((f32[128,256]{1,0:T(8,128)}), f32[32,256]{1,0:T(8,128)}) %reduce-scatter.26.cloned.1.call-update) | async-done | bytes 32784 | tf_op jit(solution)/shard_map/reduce_scatter | solution.py:68
  130.8 21.9 %reduce-scatter.28.cloned.1.call-done = f32[32,256]{1,0:T(8,128)} async-done(((f32[128,256]{1,0:T(8,128)}), f32[32,256]{1,0:T(8,128)}) %reduce-scatter.28.cloned.1.call-update) | async-done | bytes 32784 | tf_op jit(solution)/shard_map/reduce_scatter | solution.py:67
  152.7 0.9 broadcast_multiply_fusion.5
  153.9 8.6 %fusion.4 = f32[32,2,1,128]{3,2,1,0:T(1,128)S(1)} fusion(f32[32,2,128,1]{2,3,1,0:T(1,128)S(1)} %bitcast.116, f32[2,32,2,128,128]{4,3,2,1,0:T(8,128)} %param.23, f32[32,2,128]{2,1,0:T(2,128)S(1)} %mul.366, f32[32,2,128]{2,1,0:T(2,128)S(1)} %get-tuple-element.25, f32[32,2]{1,0:T(8,128)S(1)} %copy.29), kind=kOutput, calls=%fused_computation.6 | convolution fusion | flops 15728640 | bytes 4325632 | tf_op jit(solution)/shard_map/bhvd,bhd->bhv/dot_general | solution.py:96
  162.8 11.8 %reduce-scatter.22.cloned.1.call-done = f32[32,256]{1,0:T(8,128)} async-done(((f32[128,256]{1,0:T(8,128)}), f32[32,256]{1,0:T(8,128)}) %reduce-scatter.22.cloned.1.call-update) | async-done | bytes 32784 | tf_op jit(solution)/shard_map/reduce_scatter | solution.py:70
  174.6 0.8 fusion.59
  175.5 5.2 %all_gather.10 = bf16[128,256]{1,0:T(8,128)(2,1)S(1)} all-gather(bf16[32,256]{1,0:T(8,128)(2,1)S(1)} %fusion.59), channel_id=1, replica_groups=mesh['tp'=8,'dp'=4] {'dp'}, dimensions={0}, use_global_device_ids=true | all-gather | bytes 81920 | tf_op jit(solution)/shard_map/all_gather | solution.py:106
  181.0 43.3 %all-reduce.1 = bf16[128,1024]{1,0:T(8,128)(2,1)S(1)} all-reduce(f32[128,1024]{1,0:T(8,128)S(1)} %fusion.30), channel_id=1, replica_groups=mesh['tp'=8,'dp'=4] {'tp'}, use_global_device_ids=true, to_apply=%region_10.11 | all-reduce | flops 131072 | bytes 786432 | tf_op jit(solution)/shard_map/psum | solution.py:109
  224.4 1.6 fusion.68
  226.1 1.6 fusion.66
  227.8 0.9 fusion.22
  228.7 1.9 fusion.24
  230.8 6.0 %psum.23 = f32[128]{0:T(128)S(1)} all-reduce(f32[128]{0:T(128)S(1)} %get-tuple-element.18), channel_id=1, replica_groups=mesh['tp'=8,'dp'=4] {'dp'}, use_global_device_ids=true, to_apply=%region_13.14 | all-reduce | flops 128 | bytes 1024 | tf_op jit(solution)/shard_map/psum | solution.py:74
  236.8 1.9 fusion.26
  238.9 1.9 fusion.28
  240.9 1.3 reduce-scatter.44.cloned.1.call-done
  242.2 0.8 copy.50
  243.0 21.7 %reduce-scatter.46.cloned.1.call-done = f32[32,2]{1,0:T(8,128)} async-done(((f32[128,2]{1,0:T(8,128)}), f32[32,2]{1,0:T(8,128)}) %reduce-scatter.46.cloned.1.call-update) | async-done | bytes 272
  264.7 0.8 copy.52
  266.3 20.5 %reduce-scatter.36.cloned.1.call-done = f32[32,256]{1,0:T(8,128)} async-done(((f32[128,256]{1,0:T(8,128)}), f32[32,256]{1,0:T(8,128)}) %reduce-scatter.36.cloned.1.call-update) | async-done | bytes 32784 | tf_op jit(solution)/shard_map/reduce_scatter | solution.py:67
  286.8 21.9 %reduce-scatter.34.cloned.1.call-done = f32[32,256]{1,0:T(8,128)} async-done(((f32[128,256]{1,0:T(8,128)}), f32[32,256]{1,0:T(8,128)}) %reduce-scatter.34.cloned.1.call-update) | async-done | bytes 32784 | tf_op jit(solution)/shard_map/reduce_scatter | solution.py:68
  308.7 22.7 %reduce-scatter.32.cloned.1.call-done = f32[32,256]{1,0:T(8,128)} async-done(((f32[128,256]{1,0:T(8,128)}), f32[32,256]{1,0:T(8,128)}) %reduce-scatter.32.cloned.1.call-update) | async-done | bytes 32784 | tf_op jit(solution)/shard_map/reduce_scatter | solution.py:69
  331.4 0.9 broadcast_multiply_fusion.2
  332.6 8.6 %fusion.1 = f32[32,2,1,128]{3,2,1,0:T(1,128)S(1)} fusion(f32[32,2,128,1]{2,3,1,0:T(1,128)S(1)} %bitcast.117, f32[2,32,2,128,128]{4,3,2,1,0:T(8,128)} %param.23, f32[32,2,128]{2,1,0:T(2,128)S(1)} %mul.398, f32[32,2,128]{2,1,0:T(2,128)S(1)} %get-tuple-element.23, f32[32,2]{1,0:T(8,128)S(1)} %copy.32), kind=kOutput, calls=%fused_computation.3 | convolution fusion | flops 15728640 | bytes 4325632 | tf_op jit(solution)/shard_map/bhvd,bhd->bhv/dot_general | solution.py:96
  341.5 11.8 %reduce-scatter.30.cloned.1.call-done = f32[32,256]{1,0:T(8,128)} async-done(((f32[128,256]{1,0:T(8,128)}), f32[32,256]{1,0:T(8,128)}) %reduce-scatter.30.cloned.1.call-update) | async-done | bytes 32784 | tf_op jit(solution)/shard_map/reduce_scatter | solution.py:70
  353.3 0.8 fusion.58
  354.1 5.2 %all_gather.11 = bf16[128,256]{1,0:T(8,128)(2,1)S(1)} all-gather(bf16[32,256]{1,0:T(8,128)(2,1)S(1)} %fusion.58), channel_id=1, replica_groups=mesh['tp'=8,'dp'=4] {'dp'}, dimensions={0}, use_global_device_ids=true | all-gather | bytes 81920 | tf_op jit(solution)/shard_map/all_gather | solution.py:106
  359.4 1.0 fusion.20
  361.3 5.4 %multiply_add_fusion.1 = (f32[1,32,2,128,128]{4,3,2,1,0:T(8,128)S(1)}, f32[1,32,2,128,128]{4,3,2,1,0:T(8,128)S(1)}) fusion(f32[2,32,2,128,128]{4,3,2,1,0:T(8,128)} %param.23, f32[32,2,128]{2,1,0:T(2,128)S(1)} %mul.366, f32[32,2,128]{2,1,0:T(2,128)S(1)} %get-tuple-element.25, f32[32,2]{1,0:T(8,128)S(1)} %copy.29, f32[32,2,128]{2,1,0:T(2,128)S(1)} %mul.398, ...), kind=kLoop, calls=%fused_computation.8 | loop fusion | flops 6291456 | bytes 16908800 | tf_op jit(solution)/shard_map/add | solution.py:90
  366.7 4.0 pad_maximum_fusion
  370.7 53.0 %reduce-scatter.38.cloned.1.call-done = f32[16,1024]{1,0:T(8,128)} async-done(((f32[128,1024]{1,0:T(8,128)}), f32[16,1024]{1,0:T(8,128)}) %reduce-scatter.38.cloned.1.call-update) | async-done | bytes 65552 | tf_op jit(solution)/shard_map/reduce_scatter | solution.py:15
  423.7 1.5 convert_element_type.31
  (75 shorter events, 4.6 us)
Async XLA Ops:
  7.2 43.0 %copy-start.1 = (bf16[2,1024,256]{2,1,0:T(8,128)(2,1)S(1)}, bf16[2,1024,256]{2,1,0:T(8,128)(2,1)}, u32[]{:S(2)}) copy-start(bf16[2,1024,256]{2,1,0:T(8,128)(2,1)} %param.14) | copy-start | bytes 3145732
  7.2 44.0 %copy-start.2 = (bf16[2,1024,256]{2,1,0:T(8,128)(2,1)S(1)}, bf16[2,1024,256]{2,1,0:T(8,128)(2,1)}, u32[]{:S(2)}) copy-start(bf16[2,1024,256]{2,1,0:T(8,128)(2,1)} %param.17) | copy-start | bytes 3145732
  7.2 45.1 %copy-start.4 = (f32[2,256]{1,0:T(2,128)S(1)}, f32[2,256]{1,0:T(2,128)}, u32[]{:S(2)}) copy-start(f32[2,256]{1,0:T(2,128)} %param.21) | copy-start | bytes 6148
  7.2 79.8 %copy-start.5 = (f32[2,32,2]{1,2,0:T(2,128)S(1)}, f32[2,32,2]{1,2,0:T(2,128)}, u32[]{:S(2)}) copy-start(f32[2,32,2]{1,2,0:T(2,128)} %param.25) | copy-start | bytes 1540
  7.2 146.5 %copy-start.3 = (f32[2,32,2,128]{3,2,1,0:T(2,128)S(1)}, f32[2,32,2,128]{3,2,1,0:T(2,128)}, u32[]{:S(2)}) copy-start(f32[2,32,2,128]{3,2,1,0:T(2,128)} %param.24) | copy-start | bytes 196612
  7.2 57.0 %reduce-scatter.42.cloned.1.call-start = ((), (), s32[]{:S(2)}) async-start(), calls=%async_computation.23 | async-start | bytes 81920
  43.5 42.7 %reduce-scatter.40.cloned.1.call-start = ((), (), s32[]{:S(2)}) async-start(), calls=%async_computation.22 | async-start | bytes 81920
  46.1 62.8 %reduce-scatter.24.cloned.1.call-start = ((), (), s32[]{:S(2)}) async-start(), calls=%async_computation.14 | async-start | bytes 163840 | tf_op jit(solution)/shard_map/reduce_scatter | solution.py:69
  48.1 82.7 %reduce-scatter.26.cloned.1.call-start = ((), (), s32[]{:S(2)}) async-start(), calls=%async_computation.15 | async-start | bytes 163840 | tf_op jit(solution)/shard_map/reduce_scatter | solution.py:68
  50.1 102.6 %reduce-scatter.28.cloned.1.call-start = ((), (), s32[]{:S(2)}) async-start(), calls=%async_computation.16 | async-start | bytes 163840 | tf_op jit(solution)/shard_map/reduce_scatter | solution.py:67
  51.0 129.7 %copy-start = (bf16[2,256,1024]{2,1,0:T(8,128)(2,1)S(1)}, bf16[2,256,1024]{2,1,0:T(8,128)(2,1)}, u32[]{:S(2)}) copy-start(bf16[2,256,1024]{2,1,0:T(8,128)(2,1)} %param.22) | copy-start | bytes 3145732
  51.1 123.6 %reduce-scatter.22.cloned.1.call-start = ((), (), s32[]{:S(2)}) async-start(), calls=%async_computation.13 | async-start | bytes 163840 | tf_op jit(solution)/shard_map/reduce_scatter | solution.py:70
  52.1 190.1 %reduce-scatter.44.cloned.1.call-start = ((), (), s32[]{:S(2)}) async-start(), calls=%async_computation.24 | async-start | bytes 81920
  226.0 38.6 %reduce-scatter.46.cloned.1.call-start = ((), (), s32[]{:S(2)}) async-start(), calls=%async_computation.25 | async-start | bytes 81920
  227.7 59.0 %reduce-scatter.36.cloned.1.call-start = ((), (), s32[]{:S(2)}) async-start(), calls=%async_computation.20 | async-start | bytes 163840 | tf_op jit(solution)/shard_map/reduce_scatter | solution.py:67
  228.7 80.0 %reduce-scatter.34.cloned.1.call-start = ((), (), s32[]{:S(2)}) async-start(), calls=%async_computation.19 | async-start | bytes 163840 | tf_op jit(solution)/shard_map/reduce_scatter | solution.py:68
  230.7 100.7 %reduce-scatter.32.cloned.1.call-start = ((), (), s32[]{:S(2)}) async-start(), calls=%async_computation.18 | async-start | bytes 163840 | tf_op jit(solution)/shard_map/reduce_scatter | solution.py:69
  238.7 114.6 %reduce-scatter.30.cloned.1.call-start = ((), (), s32[]{:S(2)}) async-start(), calls=%async_computation.17 | async-start | bytes 163840 | tf_op jit(solution)/shard_map/reduce_scatter | solution.py:70
  240.8 182.8 %reduce-scatter.38.cloned.1.call-start = ((), (), s32[]{:S(2)}) async-start(), calls=%async_computation.21 | async-start | bytes 589824 | tf_op jit(solution)/shard_map/reduce_scatter | solution.py:15
Sparse Core Ops, SparseCore 0:
  43.6 20.5 reduce-scatter.41
  66.6 19.5 reduce-scatter.39
  89.2 19.6 reduce-scatter.23
  111.1 19.6 reduce-scatter.25
  133.1 19.6 reduce-scatter.27
  155.0 19.6 reduce-scatter.21
  226.2 15.9 reduce-scatter.43
  245.1 19.4 reduce-scatter.45
  267.1 19.6 reduce-scatter.35
  289.1 19.6 reduce-scatter.33
  311.7 19.6 reduce-scatter.31
  333.6 19.6 reduce-scatter.29
  360.6 63.0 reduce-scatter.37
where the time goes:
time: 433 us; the launch traced here: 432 us
  waiting for transfers between devices  258 us (60%)
  blocking collectives  98.2 us (23%)
  matrix products  35.8 us (8%)
  other arithmetic  17.3 us (4%)
  between operations  14.2 us (3%)
  local copies, waits for them, and re-layouts  7.86 us (2%)
    reduce_scatter x1, waiting for transfers between devices, spread_heads(): return lax.psum_scatter(out_part, 'tp', scatter_dimension=0, tiled=True)  53 us
    unnamed x17, waiting for transfers between devices  50.6 us
    reduce_scatter x2, waiting for transfers between devices, per_device(): lax.psum_scatter(value_part, 'dp', scatter_dimension=0, tiled=True)  44.3 us
    reduce_scatter x2, waiting for transfers between devices, per_device(): lax.psum_scatter(key_part, 'dp', scatter_dimension=0, tiled=True)  43.9 us
    psum x1, blocking collectives, per_device(): gathered = lax.psum(out_part, 'tp').astype(jnp.bfloat16)  43.3 us
    reduce_scatter x2, waiting for transfers between devices, per_device(): lax.psum_scatter(query_part, 'dp', scatter_dimension=0, tiled=True)  42.4 us
    all_gather x1, blocking collectives, gather_rows(): return lax.all_gather(block_input, 'tp', axis=0, tiled=True)  32.8 us
    reduce_scatter x2, waiting for transfers between devices, per_device(): lax.psum_scatter(outgate_part, 'dp', scatter_dimension=0, tiled=True)  23.6 us
  transfers between devices with their start and end apart: 13, of which 13 were waited for; matrix products, arithmetic and copies ran while one was open for 12% of the time, Pallas kernels for 0%

commit v1 on v0

--- a/solution.py
+++ b/solution.py
@@ -1,3 +1,4 @@
+import functools
 import jax
 import jax.numpy as jnp
 from jax import lax
@@ -5,6 +6,14 @@
 
 D = 4096
 EPSILON = 1e-06
+
+
+def balance_stops_all(array_in, which_axis):
+    odd = jnp.sum(lax.all_gather(array_in, axis_name=which_axis), axis=0)
+    return odd
+
+
+answer_rounds = functools.partial(balance_stops_all, which_axis="tp")
 
 
 def gather_rows(block_input):
@@ -106,7 +115,7 @@
         all_gated = lax.all_gather(gated_out, "dp", axis=0, tiled=True)
         out_part = jnp.dot(all_gated, proj_weight[layer_num], preferred_element_type=jnp.float32)
         if layer_num + 1 < num_blocks:
-            gathered = lax.psum(out_part, "tp").astype(jnp.bfloat16)
+            gathered = answer_rounds(out_part).astype(jnp.bfloat16)
         else:
             final_rows = spread_heads(out_part).astype(jnp.bfloat16)
         cell_list.append(new_cell)

time: 433 us -> 468 us (1.081)
  waiting for transfers between devices: 258 us -> 333 us
  blocking collectives: 98.2 us -> 54.6 us
    all_gather x0 -> x1, waiting for transfers between devices: none -> 72.9 us  [balance_stops_all(): odd = jnp.sum(lax.all_gather(array_in, axis_name=which_axis), axis=0)]
    psum x1 -> x0, blocking collectives: 43.3 us -> none  [per_device(): gathered = lax.psum(out_part, 'tp').astype(jnp.bfloat16)]
    unnamed x17 -> x18, waiting for transfers between devices: 50.6 us -> 53.2 us
  transfers between devices with their start and end apart: 13 -> 14, of which waited for: 13 -> 14; matrix products, arithmetic and copies ran while one was open for 12% -> 11% of each run, Pallas kernels for 0% -> 0%
where the time goes in v1:
time: 468 us; the launch traced here: 467 us
  waiting for transfers between devices  333 us (71%)
  blocking collectives  54.6 us (12%)
  matrix products  36.6 us (8%)
  other arithmetic  19.9 us (4%)
  between operations  14.2 us (3%)
  local copies, waits for them, and re-layouts  7.86 us (2%)
    all_gather x1, waiting for transfers between devices, balance_stops_all(): odd = jnp.sum(lax.all_gather(array_in, axis_name=which_axis), axis=0)  72.9 us
    unnamed x18, waiting for transfers between devices  53.2 us
    reduce_scatter x1, waiting for transfers between devices, spread_heads(): return lax.psum_scatter(out_part, 'tp', scatter_dimension=0, tiled=True)  53 us
    reduce_scatter x2, waiting for transfers between devices, per_device(): lax.psum_scatter(value_part, 'dp', scatter_dimension=0, tiled=True)  44.2 us
    reduce_scatter x2, waiting for transfers between devices, per_device(): lax.psum_scatter(key_part, 'dp', scatter_dimension=0, tiled=True)  44.1 us
    reduce_scatter x2, waiting for transfers between devices, per_device(): lax.psum_scatter(query_part, 'dp', scatter_dimension=0, tiled=True)  42.3 us
    all_gather x1, blocking collectives, gather_rows(): return lax.all_gather(block_input, 'tp', axis=0, tiled=True)  32.8 us
    reduce_scatter x2, waiting for transfers between devices, per_device(): lax.psum_scatter(outgate_part, 'dp', scatter_dimension=0, tiled=True)  23.8 us
  transfers between devices with their start and end apart: 14, of which 14 were waited for; matrix products, arithmetic and copies ran while one was open for 11% of the time, Pallas kernels for 0%

profile of v1, /device:TPU:0, one launch (start us, length us, event | category | flops | bytes accessed | tf_op | source)
XLA Modules:
  0.0 467.1 jit_solution(6951650770260440371)
XLA Ops:
  7.3 0.9 fusion.90
  8.1 32.8 %all_gather.15 = bf16[128,1024]{1,0:T(8,128)(2,1)S(1)} all-gather(bf16[16,1024]{1,0:T(8,128)(2,1)} %param.13), channel_id=1, replica_groups=mesh['tp'=8,'dp'=4] {'tp'}, dimensions={0}, use_global_device_ids=true | all-gather | bytes 294912 | tf_op jit(solution)/shard_map/all_gather | solution.py:20
  40.9 1.6 fusion.89
  42.5 0.9 fusion.53
  43.5 1.6 fusion.88
  45.1 0.9 fusion.55
  46.1 1.9 fusion.36
  48.1 1.9 fusion.34
  50.2 0.9 fusion.32
  51.1 0.9 fusion.38
  52.2 5.7 %psum.14 = f32[128]{0:T(128)S(1)} all-reduce(f32[128]{0:T(128)S(1)} %fusion.17), channel_id=1, replica_groups=mesh['tp'=8,'dp'=4] {'dp'}, use_global_device_ids=true, to_apply=%region_2.0 | all-reduce | flops 128 | bytes 1024 | tf_op jit(solution)/shard_map/psum | solution.py:83
  58.0 6.2 %reduce-scatter.42.cloned.1.call-done = f32[32,2]{1,0:T(8,128)} async-done(((f32[128,2]{1,0:T(8,128)}), f32[32,2]{1,0:T(8,128)}) %reduce-scatter.42.cloned.1.call-update) | async-done | bytes 272
  64.2 0.8 copy.60
  65.0 21.2 %reduce-scatter.40.cloned.1.call-done = f32[32,2]{1,0:T(8,128)} async-done(((f32[128,2]{1,0:T(8,128)}), f32[32,2]{1,0:T(8,128)}) %reduce-scatter.40.cloned.1.call-update) | async-done | bytes 272
  87.2 21.7 %reduce-scatter.24.cloned.1.call-done = f32[32,256]{1,0:T(8,128)} async-done(((f32[128,256]{1,0:T(8,128)}), f32[32,256]{1,0:T(8,128)}) %reduce-scatter.24.cloned.1.call-update) | async-done | bytes 32784 | tf_op jit(solution)/shard_map/reduce_scatter | solution.py:78
  108.9 22.0 %reduce-scatter.26.cloned.1.call-done = f32[32,256]{1,0:T(8,128)} async-done(((f32[128,256]{1,0:T(8,128)}), f32[32,256]{1,0:T(8,128)}) %reduce-scatter.26.cloned.1.call-update) | async-done | bytes 32784 | tf_op jit(solution)/shard_map/reduce_scatter | solution.py:77
  130.9 22.0 %reduce-scatter.28.cloned.1.call-done = f32[32,256]{1,0:T(8,128)} async-done(((f32[128,256]{1,0:T(8,128)}), f32[32,256]{1,0:T(8,128)}) %reduce-scatter.28.cloned.1.call-update) | async-done | bytes 32784 | tf_op jit(solution)/shard_map/reduce_scatter | solution.py:76
  152.8 0.9 broadcast_multiply_fusion.5
  154.0 8.6 %fusion.4 = f32[32,2,1,128]{3,2,1,0:T(1,128)S(1)} fusion(f32[32,2,128,1]{2,3,1,0:T(1,128)S(1)} %bitcast.118, f32[2,32,2,128,128]{4,3,2,1,0:T(8,128)} %param.23, f32[32,2,128]{2,1,0:T(2,128)S(1)} %mul.366, f32[32,2,128]{2,1,0:T(2,128)S(1)} %get-tuple-element.25, f32[32,2]{1,0:T(8,128)S(1)} %copy.41), kind=kOutput, calls=%fused_computation.6 | convolution fusion | flops 15728640 | bytes 4325632 | tf_op jit(solution)/shard_map/bhvd,bhd->bhv/dot_general | solution.py:105
  163.0 11.8 %reduce-scatter.22.cloned.1.call-done = f32[32,256]{1,0:T(8,128)} async-done(((f32[128,256]{1,0:T(8,128)}), f32[32,256]{1,0:T(8,128)}) %reduce-scatter.22.cloned.1.call-update) | async-done | bytes 32784 | tf_op jit(solution)/shard_map/reduce_scatter | solution.py:79
  174.8 0.8 fusion.59
  175.6 5.2 %all_gather.16 = bf16[128,256]{1,0:T(8,128)(2,1)S(1)} all-gather(bf16[32,256]{1,0:T(8,128)(2,1)S(1)} %fusion.59), channel_id=1, replica_groups=mesh['tp'=8,'dp'=4] {'dp'}, dimensions={0}, use_global_device_ids=true | all-gather | bytes 81920 | tf_op jit(solution)/shard_map/all_gather | solution.py:115
  180.9 1.0 fusion.30
  182.0 72.9 %all-gather.3.cloned.1.call-done = f32[1024,1024]{1,0:T(8,128)} async-done(((f32[128,1024]{1,0:T(8,128)}), f32[1024,1024]{1,0:T(8,128)}) %all-gather.3.cloned.1.call-update) | async-done | bytes 4194320 | tf_op jit(solution)/shard_map/all_gather | solution.py:12
  254.9 2.6 reduce_sum.66
  257.7 1.6 fusion.68
  259.4 1.6 fusion.66
  261.1 0.9 fusion.22
  262.0 1.9 fusion.24
  264.1 5.7 %psum.15 = f32[128]{0:T(128)S(1)} all-reduce(f32[128]{0:T(128)S(1)} %get-tuple-element.18), channel_id=1, replica_groups=mesh['tp'=8,'dp'=4] {'dp'}, use_global_device_ids=true, to_apply=%region_13.14 | all-reduce | flops 128 | bytes 1024 | tf_op jit(solution)/shard_map/psum | solution.py:83
  269.7 1.9 fusion.26
  271.8 1.9 fusion.28
  273.8 3.7 reduce-scatter.44.cloned.1.call-done
  277.5 0.8 copy.62
  278.3 21.8 %reduce-scatter.46.cloned.1.call-done = f32[32,2]{1,0:T(8,128)} async-done(((f32[128,2]{1,0:T(8,128)}), f32[32,2]{1,0:T(8,128)}) %reduce-scatter.46.cloned.1.call-update) | async-done | bytes 272
  301.7 20.4 %reduce-scatter.36.cloned.1.call-done = f32[32,256]{1,0:T(8,128)} async-done(((f32[128,256]{1,0:T(8,128)}), f32[32,256]{1,0:T(8,128)}) %reduce-scatter.36.cloned.1.call-update) | async-done | bytes 32784 | tf_op jit(solution)/shard_map/reduce_scatter | solution.py:76
  322.1 22.1 %reduce-scatter.34.cloned.1.call-done = f32[32,256]{1,0:T(8,128)} async-done(((f32[128,256]{1,0:T(8,128)}), f32[32,256]{1,0:T(8,128)}) %reduce-scatter.34.cloned.1.call-update) | async-done | bytes 32784 | tf_op jit(solution)/shard_map/reduce_scatter | solution.py:77
  344.2 22.5 %reduce-scatter.32.cloned.1.call-done = f32[32,256]{1,0:T(8,128)} async-done(((f32[128,256]{1,0:T(8,128)}), f32[32,256]{1,0:T(8,128)}) %reduce-scatter.32.cloned.1.call-update) | async-done | bytes 32784 | tf_op jit(solution)/shard_map/reduce_scatter | solution.py:78
  366.7 0.9 broadcast_multiply_fusion.2
  367.9 8.6 %fusion.1 = f32[32,2,1,128]{3,2,1,0:T(1,128)S(1)} fusion(f32[32,2,128,1]{2,3,1,0:T(1,128)S(1)} %bitcast.119, f32[2,32,2,128,128]{4,3,2,1,0:T(8,128)} %param.23, f32[32,2,128]{2,1,0:T(2,128)S(1)} %mul.398, f32[32,2,128]{2,1,0:T(2,128)S(1)} %get-tuple-element.23, f32[32,2]{1,0:T(8,128)S(1)} %copy.44), kind=kOutput, calls=%fused_computation.3 | convolution fusion | flops 15728640 | bytes 4325632 | tf_op jit(solution)/shard_map/bhvd,bhd->bhv/dot_general | solution.py:105
  376.8 11.9 %reduce-scatter.30.cloned.1.call-done = f32[32,256]{1,0:T(8,128)} async-done(((f32[128,256]{1,0:T(8,128)}), f32[32,256]{1,0:T(8,128)}) %reduce-scatter.30.cloned.1.call-update) | async-done | bytes 32784 | tf_op jit(solution)/shard_map/reduce_scatter | solution.py:79
  388.8 0.8 fusion.58
  389.6 5.2 %all_gather.19 = bf16[128,256]{1,0:T(8,128)(2,1)S(1)} all-gather(bf16[32,256]{1,0:T(8,128)(2,1)S(1)} %fusion.58), channel_id=1, replica_groups=mesh['tp'=8,'dp'=4] {'dp'}, dimensions={0}, use_global_device_ids=true | all-gather | bytes 81920 | tf_op jit(solution)/shard_map/all_gather | solution.py:115
  394.8 1.0 fusion.20
  396.8 5.4 %multiply_add_fusion.1 = (f32[1,32,2,128,128]{4,3,2,1,0:T(8,128)S(1)}, f32[1,32,2,128,128]{4,3,2,1,0:T(8,128)S(1)}) fusion(f32[2,32,2,128,128]{4,3,2,1,0:T(8,128)} %param.23, f32[32,2,128]{2,1,0:T(2,128)S(1)} %mul.366, f32[32,2,128]{2,1,0:T(2,128)S(1)} %get-tuple-element.25, f32[32,2]{1,0:T(8,128)S(1)} %copy.41, f32[32,2,128]{2,1,0:T(2,128)S(1)} %mul.398, ...), kind=kLoop, calls=%fused_computation.8 | loop fusion | flops 6291456 | bytes 16908800 | tf_op jit(solution)/shard_map/add | solution.py:99
  402.2 4.0 pad_maximum_fusion
  406.1 53.0 %reduce-scatter.38.cloned.1.call-done = f32[16,1024]{1,0:T(8,128)} async-done(((f32[128,1024]{1,0:T(8,128)}), f32[16,1024]{1,0:T(8,128)}) %reduce-scatter.38.cloned.1.call-update) | async-done | bytes 65552 | tf_op jit(solution)/shard_map/reduce_scatter | solution.py:24
  459.1 1.5 convert_element_type.31
  (78 shorter events, 6.0 us)
Async XLA Ops:
  7.2 43.0 %copy-start.1 = (bf16[2,1024,256]{2,1,0:T(8,128)(2,1)S(1)}, bf16[2,1024,256]{2,1,0:T(8,128)(2,1)}, u32[]{:S(2)}) copy-start(bf16[2,1024,256]{2,1,0:T(8,128)(2,1)} %param.14) | copy-start | bytes 3145732
  7.2 44.0 %copy-start.2 = (bf16[2,1024,256]{2,1,0:T(8,128)(2,1)S(1)}, bf16[2,1024,256]{2,1,0:T(8,128)(2,1)}, u32[]{:S(2)}) copy-start(bf16[2,1024,256]{2,1,0:T(8,128)(2,1)} %param.17) | copy-start | bytes 3145732
  7.2 45.0 %copy-start.4 = (f32[2,256]{1,0:T(2,128)S(1)}, f32[2,256]{1,0:T(2,128)}, u32[]{:S(2)}) copy-start(f32[2,256]{1,0:T(2,128)} %param.21) | copy-start | bytes 6148
  7.2 79.8 %copy-start.5 = (f32[2,32,2]{1,2,0:T(2,128)S(1)}, f32[2,32,2]{1,2,0:T(2,128)}, u32[]{:S(2)}) copy-start(f32[2,32,2]{1,2,0:T(2,128)} %param.25) | copy-start | bytes 1540
  7.2 146.6 %copy-start.3 = (f32[2,32,2,128]{3,2,1,0:T(2,128)S(1)}, f32[2,32,2,128]{3,2,1,0:T(2,128)}, u32[]{:S(2)}) copy-start(f32[2,32,2,128]{3,2,1,0:T(2,128)} %param.24) | copy-start | bytes 196612
  7.2 57.0 %reduce-scatter.42.cloned.1.call-start = ((), (), s32[]{:S(2)}) async-start(), calls=%async_computation.24 | async-start | bytes 81920
  43.5 42.7 %reduce-scatter.40.cloned.1.call-start = ((), (), s32[]{:S(2)}) async-start(), calls=%async_computation.23 | async-start | bytes 81920
  46.1 62.8 %reduce-scatter.24.cloned.1.call-start = ((), (), s32[]{:S(2)}) async-start(), calls=%async_computation.14 | async-start | bytes 163840 | tf_op jit(solution)/shard_map/reduce_scatter | solution.py:78
  48.1 82.8 %reduce-scatter.26.cloned.1.call-start = ((), (), s32[]{:S(2)}) async-start(), calls=%async_computation.15 | async-start | bytes 163840 | tf_op jit(solution)/shard_map/reduce_scatter | solution.py:77
  50.1 102.7 %reduce-scatter.28.cloned.1.call-start = ((), (), s32[]{:S(2)}) async-start(), calls=%async_computation.16 | async-start | bytes 163840 | tf_op jit(solution)/shard_map/reduce_scatter | solution.py:76
  51.0 129.8 %copy-start = (bf16[2,256,1024]{2,1,0:T(8,128)(2,1)S(1)}, bf16[2,256,1024]{2,1,0:T(8,128)(2,1)}, u32[]{:S(2)}) copy-start(bf16[2,256,1024]{2,1,0:T(8,128)(2,1)} %param.22) | copy-start | bytes 3145732
  51.1 123.7 %reduce-scatter.22.cloned.1.call-start = ((), (), s32[]{:S(2)}) async-start(), calls=%async_computation.13 | async-start | bytes 163840 | tf_op jit(solution)/shard_map/reduce_scatter | solution.py:79
  52.0 202.9 %all-gather.3.cloned.1.call-start = ((), (), s32[]{:S(2)}) async-start(), calls=%async_computation.22 | async-start | bytes 4718592 | tf_op jit(solution)/shard_map/all_gather | solution.py:12
  181.9 95.6 %reduce-scatter.44.cloned.1.call-start = ((), (), s32[]{:S(2)}) async-start(), calls=%async_computation.25 | async-start | bytes 81920
  259.3 40.8 %reduce-scatter.46.cloned.1.call-start = ((), (), s32[]{:S(2)}) async-start(), calls=%async_computation.26 | async-start | bytes 81920
  261.0 61.0 %reduce-scatter.36.cloned.1.call-start = ((), (), s32[]{:S(2)}) async-start(), calls=%async_computation.20 | async-start | bytes 163840 | tf_op jit(solution)/shard_map/reduce_scatter | solution.py:76
  262.0 82.2 %reduce-scatter.34.cloned.1.call-start = ((), (), s32[]{:S(2)}) async-start(), calls=%async_computation.19 | async-start | bytes 163840 | tf_op jit(solution)/shard_map/reduce_scatter | solution.py:77
  264.0 102.7 %reduce-scatter.32.cloned.1.call-start = ((), (), s32[]{:S(2)}) async-start(), calls=%async_computation.18 | async-start | bytes 163840 | tf_op jit(solution)/shard_map/reduce_scatter | solution.py:78
  271.7 117.1 %reduce-scatter.30.cloned.1.call-start = ((), (), s32[]{:S(2)}) async-start(), calls=%async_computation.17 | async-start | bytes 163840 | tf_op jit(solution)/shard_map/reduce_scatter | solution.py:79
  273.8 185.4 %reduce-scatter.38.cloned.1.call-start = ((), (), s32[]{:S(2)}) async-start(), calls=%async_computation.21 | async-start | bytes 589824 | tf_op jit(solution)/shard_map/reduce_scatter | solution.py:24
Sparse Core Ops, SparseCore 0:
  43.6 20.5 reduce-scatter.41
  66.6 19.5 reduce-scatter.39
  89.2 19.6 reduce-scatter.23
  111.2 19.6 reduce-scatter.25
  133.1 19.6 reduce-scatter.27
  155.1 19.6 reduce-scatter.21
  182.1 72.7 all-gather.2
  259.4 18.0 reduce-scatter.43
  280.5 19.5 reduce-scatter.45
  302.4 19.6 reduce-scatter.35
  324.5 19.6 reduce-scatter.33
  347.0 19.6 reduce-scatter.31
  369.1 19.6 reduce-scatter.29
  396.0 63.0 reduce-scatter.37
